TPU v7x, 512 devices: a whole 4x8x8 slice. The times are simulated.
512 devices in a mesh: ep: 128 (over z, y, core), tp: 4 (over x).
Axes of the slice: x: 4, y: 8, z: 8, core: 2. Of those that a mesh axis runs over, the one named last changes fastest.
Arguments:
- tokens: bfloat16 [2048, 2048], P('ep'), may hold values from -6 to 6
- head_state: float32 [2048, 16, 4096], P('ep', 'tp'), may hold values from -6 to 6
- mixer_gain: float32 [2048], replicated, may hold values from 0.1 to 1.9
- w_query: bfloat16 [2048, 1024], P('ep', 'tp'), may hold values from -0.125 to 0.125
- w_key: bfloat16 [2048, 1024], P('ep', 'tp'), may hold values from -0.125 to 0.125
- w_value: bfloat16 [2048, 1024], P('ep', 'tp'), may hold values from -0.125 to 0.125
- decay_down: bfloat16 [2048, 64], replicated, may hold values from -0.125 to 0.125
- decay_up: bfloat16 [64, 1024], replicated, may hold values from -3 to 3
- decay_base: float32 [1024], P('tp'), may hold values from -4 to 0
- rate_down: bfloat16 [2048, 64], replicated, may hold values from -0.125 to 0.125
- rate_up: bfloat16 [64, 1024], replicated, may hold values from -0.75 to 0.75
- head_gain: float32 [1024], P('tp'), may hold values from 0.1 to 1.9
- w_out: bfloat16 [1024, 2048], P('tp', 'ep'), may hold values from -0.1875 to 0.1875
- expert_gain: float32 [2048], replicated, may hold values from 0.1 to 1.9
- expert_ids: int32 [2048, 2], P('ep'), may hold values from 0 to 127, all different within a row; in each aligned block of 16 rows (0 to 15, 16 to 31, ...) at most 1 rows name the same one
- route_weight: float32 [2048, 2], P('ep'), may hold values from 0.2 to 1
- w_gate: bfloat16 [128, 2048, 512], P('ep', None, 'tp'), may hold values from -0.125 to 0.125
- w_up: bfloat16 [128, 2048, 512], P('ep', None, 'tp'), may hold values from -0.125 to 0.125
- w_down: bfloat16 [128, 512, 2048], P('ep', 'tp'), may hold values from -0.25 to 0.25
Outputs:
- layer_out: bfloat16 [2048, 2048], P('ep', 'tp')
- next_state: float32 [2048, 16, 4096], P('ep', 'tp')
Inputs may be any that keep to these rules, and one draw needn't show every extreme that they name: `expert_ids`: each row names 2 different experts; among the 16 rows of one index of ep no expert is named more than 1 times, and in the rows of some indices one expert is named exactly 1 times.
All inputs are finite; a program needn't handle non-finite values.
Results may differ from a plain program's by a relative error of at most 0.015.
Values may be sent and summed in bfloat16 or wider, within the bound.
A program may use at most 64 MiB of HBM per device.

v0:
```python
import jax
import jax.numpy as jnp
from jax import lax
from jax.sharding import PartitionSpec as P

norm_eps = 1e-06
group_eps = 0.00064


def sent_together(arrays, axis, dim, along):
    widths = [a.shape[along] for a in arrays]
    both = jnp.concatenate(arrays, axis=along)
    out = lax.all_gather(both, axis, axis=dim, tiled=True)
    return tuple(jnp.split(out, [sum(widths[:k]) for k in range(1, len(widths))], axis=along))


def from_everyone(array, axis):
    copies = jnp.broadcast_to(array, (lax.axis_size(axis), *array.shape))
    return lax.all_to_all(copies, axis, split_axis=0, concat_axis=0, tiled=True)


def taken_together(array, axis):
    everything = from_everyone(array, axis)
    return jnp.sum(everything.astype(jnp.float32), axis=0)


def split_up(array, dim, peers):
    before, after = (array.shape[:dim], array.shape[dim + 1 :])
    return jnp.moveaxis(array.reshape(*before, peers, -1, *after), dim, 0)


def sum_at_owner(array, axis, dim):
    peers = lax.axis_size(axis)
    parts = lax.all_to_all(split_up(array, dim, peers), axis, 0, 0, tiled=True)
    return jnp.sum(parts.astype(jnp.float32), axis=0)


def rms_scale(activity, gain):
    widened = activity.astype(jnp.float32)
    scaled = widened * lax.rsqrt(jnp.mean(widened * widened, axis=-1, keepdims=True) + norm_eps)
    return (scaled * gain).astype(jnp.bfloat16)


def low_rank(normed, decay_down, decay_up, decay_base, rate_down, rate_up):
    decay_low = jnp.tanh(jnp.dot(normed, decay_down, preferred_element_type=jnp.float32)).astype(
        jnp.bfloat16
    )
    decay_pre = decay_base + jnp.dot(decay_low, decay_up, preferred_element_type=jnp.float32)
    decays = jnp.exp(-jnp.exp(-jax.nn.softplus(-decay_pre) - 0.5))
    rate_low = jnp.dot(normed, rate_down, preferred_element_type=jnp.float32).astype(jnp.bfloat16)
    rates = jax.nn.sigmoid(jnp.dot(rate_low, rate_up, preferred_element_type=jnp.float32))
    return (decays, rates)


def recurrence(queries, key_rows, value_rows, decays, rates, old_state, head_gain):
    row_count, head_count, _ = old_state.shape
    head_size = queries.shape[1] // head_count
    head_shape = (row_count, head_count, head_size)
    query_heads = queries.astype(jnp.float32).reshape(head_shape)
    key_heads = key_rows.astype(jnp.float32).reshape(head_shape)
    value_heads = value_rows.astype(jnp.float32).reshape(head_shape)
    decay_heads = decays.reshape(head_shape)
    rate_heads = rates.reshape(head_shape)
    unit_keys = key_heads * lax.rsqrt(jnp.sum(key_heads * key_heads, axis=-1, keepdims=True) + 1.0)
    state_grid = old_state.reshape(row_count, head_count, head_size, head_size)
    removed = jnp.sum(state_grid * unit_keys[:, :, None, :], axis=-1)
    updated = (
        state_grid * decay_heads[:, :, None, :]
        - removed[:, :, :, None] * (unit_keys * rate_heads)[:, :, None, :]
        + value_heads[:, :, :, None] * key_heads[:, :, None, :]
    )
    readout = jnp.sum(updated * query_heads[:, :, None, :], axis=-1)
    centred = readout - jnp.mean(readout, axis=-1, keepdims=True)
    spread = jnp.mean(centred * centred, axis=-1, keepdims=True)
    scaled = centred * lax.rsqrt(spread + group_eps) * head_gain.reshape(head_count, head_size)
    return (
        updated.reshape(row_count, head_count, head_size * head_size),
        scaled.reshape(row_count, head_count * head_size).astype(jnp.bfloat16),
    )


def body(
    tokens,
    head_state,
    mixer_gain,
    w_query,
    w_key,
    w_value,
    decay_down,
    decay_up,
    decay_base,
    rate_down,
    rate_up,
    head_gain,
    w_out,
    expert_gain,
    expert_ids,
    route_weight,
    w_gate,
    w_up,
    w_down,
):
    seq_rows, width = tokens.shape
    local_cols = w_query.shape[1]
    head_lane = lax.axis_index("tp")
    normed = rms_scale(tokens, mixer_gain)
    pieces = sent_together((w_query, w_key, w_value), "ep", 0, 1)
    projected = tuple(
        (
            jnp.dot(normed, weight_piece, preferred_element_type=jnp.float32)
            for weight_piece in pieces
        )
    )
    queries, key_rows, value_rows = (member.astype(jnp.bfloat16) for member in projected)
    col_offset = head_lane * local_cols
    decays, rates = low_rank(
        normed,
        decay_down,
        lax.dynamic_slice_in_dim(decay_up, col_offset, local_cols, 1),
        decay_base,
        rate_down,
        lax.dynamic_slice_in_dim(rate_up, col_offset, local_cols, 1),
    )
    next_state, head_out = recurrence(
        queries, key_rows, value_rows, decays, rates, head_state, head_gain
    )
    partial_out = jnp.dot(
        head_out,
        lax.all_gather(w_out, "ep", axis=1, tiled=True),
        preferred_element_type=jnp.float32,
    )
    mixed_out = taken_together(partial_out.astype(jnp.bfloat16), "tp").astype(jnp.float32)
    residual = (tokens.astype(jnp.float32) + mixed_out).astype(jnp.bfloat16)
    expert_in = rms_scale(residual, expert_gain)
    experts = lax.axis_size("ep")
    top_count = expert_ids.shape[1]
    slot_count = max(1, 2 * seq_rows * top_count // experts)
    slot_total = experts * slot_count
    flat_ids = expert_ids.reshape(-1)
    matches = (flat_ids[:, None] == jnp.arange(experts, dtype=jnp.int32)[None, :]).astype(jnp.int32)
    slot_rank = jnp.sum((jnp.cumsum(matches, axis=0) - 1) * matches, axis=1)
    slot_ids = (flat_ids * slot_count + slot_rank).reshape(seq_rows, top_count)
    slot_match = (
        slot_ids[:, :, None] == jnp.arange(slot_total, dtype=jnp.int32)[None, None, :]
    ).astype(jnp.float32)
    picker = jnp.sum(slot_match, axis=1).astype(jnp.bfloat16)
    outbound = jnp.einsum("ts,td->sd", picker, expert_in, preferred_element_type=jnp.float32)
    outbound = outbound.astype(jnp.bfloat16).reshape(experts, slot_count, expert_in.shape[1])
    gate_local, up_local, down_local = (w_gate[0], w_up[0], w_down[0])
    arrived = lax.all_to_all(outbound, "ep", split_axis=0, concat_axis=0, tiled=True)
    sources, held, _ = arrived.shape
    flat_rows = arrived.reshape(sources * held, width)
    gate_act = jnp.dot(flat_rows, gate_local, preferred_element_type=jnp.float32)
    up_act = jnp.dot(flat_rows, up_local, preferred_element_type=jnp.float32)
    hidden = (jax.nn.silu(gate_act) * up_act).astype(jnp.bfloat16)
    partial_rows = jnp.dot(hidden, down_local, preferred_element_type=jnp.float32).reshape(
        sources, held, width
    )
    reduced = sum_at_owner(partial_rows.astype(jnp.bfloat16), "tp", 2)
    returned = lax.all_to_all(
        reduced.astype(jnp.bfloat16), "ep", split_axis=0, concat_axis=0, tiled=True
    )
    shares = route_weight / jnp.sum(route_weight, axis=1, keepdims=True)
    combine = jnp.sum(slot_match * shares[:, :, None], axis=1)
    routed = jnp.dot(combine, returned.reshape(slot_total, -1).astype(jnp.float32))
    own_cols = routed.shape[1]
    kept = lax.dynamic_slice_in_dim(residual, head_lane * own_cols, own_cols, 1)
    layer_out = (kept.astype(jnp.float32) + routed).astype(jnp.bfloat16)
    return (layer_out, next_state)


def solution(mesh):
    return jax.shard_map(
        body,
        mesh=mesh,
        in_specs=(
            P("ep", None),
            P("ep", "tp", None),
            P(),
            P("ep", "tp"),
            P("ep", "tp"),
            P("ep", "tp"),
            P(),
            P(),
            P("tp"),
            P(),
            P(),
            P("tp"),
            P("tp", "ep"),
            P(),
            P("ep", None),
            P("ep", None),
            P("ep", None, "tp"),
            P("ep", None, "tp"),
            P("ep", "tp", None),
        ),
        out_specs=(P("ep", "tp"), P("ep", "tp", None)),
        check_vma=False,
    )
```

profile of v0, /device:TPU:1, one launch (start us, length us, event | category | flops | bytes accessed | tf_op | source)
XLA Modules:
  0.0 267.5 jit_solution(1612568220506573948)
XLA Ops:
  7.2 1.4 pad_maximum_fusion
  8.7 0.7 all-gather.5.cloned.1.call-update
  9.4 1.0 fusion.34
  10.4 1.4 fusion.10
  11.8 1.4 fusion.55
  13.4 2.1 reshape.119
  15.5 1.5 mul.201
  17.0 3.1 %mul.221 = f32[16,4,4096]{2,1,0:T(4,128)} reshape(f32[16,4,64,64]{3,2,1,0:T(8,128)} %mul.201) | data formatting | bytes 2097152 | tf_op jit(solution)/shard_map/mul | solution.py:68
  20.4 80.8 %all-gather.3.cloned.1.call-done = bf16[2048,768]{1,0:T(8,128)(2,1)} async-done(((bf16[16,768]{1,0:T(8,128)(2,1)}), bf16[2048,768]{1,0:T(8,128)(2,1)}) %all-gather.3.cloned.1.call-update) | async-done | bytes 3145744 | tf_op jit(solution)/shard_map/all_gather | solution.py:13
  101.2 1.5 fusion.14
  102.8 1.5 fusion.12
  104.4 1.5 fusion.13
  106.2 8.8 %broadcast_multiply_fusion = (f32[16,4,64,64]{3,2,1,0:T(8,128)}, f32[16,4,64]{2,1,0:T(4,128)S(1)}, f32[16,4,64,64]{3,2,1,0:T(8,128)}) fusion(f32[16,4,64]{2,1,0:T(4,128)S(1)} %reshape.128, f32[16,4,64]{2,1,0:T(4,128)S(1)} %reshape.129, f32[16,4,64]{2,1,0:T(4,128)S(1)} %reshape.130, f32[16,4,64,64]{3,2,1,0:T(8,128)S(1)} %reshape.119, ...), kind=kOutput, calls=%fused_computation.33 | output fusion | flops 2097215 | bytes 3260416 | tf_op jit(solution)/shard_map/mul | solution.py:69
  115.1 3.2 %mul.223 = f32[16,4,4096]{2,1,0:T(4,128)} reshape(f32[16,4,64,64]{3,2,1,0:T(8,128)} %get-tuple-element.12) | data formatting | bytes 2097152 | tf_op jit(solution)/shard_map/mul | solution.py:69
  118.2 1.8 mul.224
  120.2 1.8 mul.225
  122.0 4.1 %multiply_reduce_fusion.2 = (f32[16,4]{1,0:T(8,128)S(1)}, f32[16,4,4096]{2,1,0:T(4,128)}) fusion(f32[16,4,4096]{2,1,0:T(4,128)} %mul.225, f32[16,4,4096]{2,1,0:T(4,128)} %mul.224, f32[16,4,4096]{2,1,0:T(4,128)} %mul.223, f32[16,4,4096]{2,1,0:T(4,128)} %param.20, f32[16,4,4096]{2,1,0:T(4,128)} %mul.221), kind=kLoop, calls=%fused_computation.31 | loop fusion | flops 1310656 | bytes 6291712 | tf_op jit(solution)/shard_map/reduce_sum | solution.py:73
  126.5 54.1 %all-gather.5.cloned.1.call-done = bf16[256,2048]{0,1:T(8,128)(2,1)} async-done(((bf16[256,16]{0,1:T(8,128)(2,1)}), bf16[256,2048]{0,1:T(8,128)(2,1)}) %all-gather.5.cloned.1.call-update) | async-done | bytes 1048592 | tf_op jit(solution)/shard_map/all_gather | solution.py:129
  180.6 1.6 convolution_convert_fusion.2
  182.2 0.7 broadcast_in_dim.2
  182.9 4.0 %all-to-all-start = ((bf16[4,16,2048]{2,1,0:T(8,128)(2,1)}), bf16[4,16,2048]{2,1,0:T(8,128)(2,1)S(1)}, u32[]{:S(2)}, u32[]{:S(2)}) async-start(bf16[4,16,2048]{2,1,0:T(8,128)(2,1)} %broadcast_in_dim.2), calls=%async_computation | async-start | bytes 524288 | tf_op jit(solution)/shard_map/all_to_all | solution.py:19
  187.3 5.5 %all-to-all-done = bf16[4,16,2048]{2,1,0:T(8,128)(2,1)S(1)} async-done(((bf16[4,16,2048]{2,1,0:T(8,128)(2,1)}), bf16[4,16,2048]{2,1,0:T(8,128)(2,1)S(1)}, u32[]{:S(2)}, u32[]{:S(2)}) %all-to-all-start) | async-done | bytes 262176 | tf_op jit(solution)/shard_map/all_to_all | solution.py:19
  193.3 0.5 broadcast.118
  193.8 1.0 reduce.4
  195.2 30.2 %all_to_all.20 = bf16[128,2,1024]{2,1,0:T(2,128)(2,1)S(1)} all-to-all(bf16[128,2,1024]{2,1,0:T(2,128)(2,1)S(1)} %reshape.132), channel_id=1, replica_groups=mesh['ep'=128,'tp'=4] {'ep'}, dimensions={0} | all-to-all | bytes 1048576 | tf_op jit(solution)/shard_map/all_to_all | solution.py:150
  226.3 0.7 convolution_convert_fusion
  227.5 12.2 %all_to_all.21 = bf16[4,128,1,512]{3,1,2,0:T(8,128)(2,1)S(1)} all-to-all(bf16[4,128,1,512]{3,1,2,0:T(8,128)(2,1)S(1)} %bitcast.38), channel_id=1, replica_groups=mesh['ep'=128,'tp'=4] {'tp'}, dimensions={0} | all-to-all | bytes 1048576 | tf_op jit(solution)/shard_map/all_to_all | solution.py:34
  239.8 0.7 reduce.5
  240.5 0.7 reshape.134
  241.2 5.8 %all-to-all-start.3 = ((bf16[128,2,256]{2,1,0:T(2,128)(2,1)}), bf16[128,2,256]{2,1,0:T(2,128)(2,1)S(1)}, u32[]{:S(2)}, u32[]{:S(2)}) async-start(bf16[128,2,256]{2,1,0:T(2,128)(2,1)} %reshape.134), calls=%async_computation.3 | async-start | bytes 262144 | tf_op jit(solution)/shard_map/all_to_all | solution.py:160
  247.0 12.8 %all-to-all-done.3 = bf16[128,2,256]{2,1,0:T(2,128)(2,1)S(1)} async-done(((bf16[128,2,256]{2,1,0:T(2,128)(2,1)}), bf16[128,2,256]{2,1,0:T(2,128)(2,1)S(1)}, u32[]{:S(2)}, u32[]{:S(2)}) %all-to-all-start.3) | async-done | bytes 131104 | tf_op jit(solution)/shard_map/all_to_all | solution.py:160
  259.9 0.8 fusion.7
  (60 shorter events, 4.4 us)
Async XLA Ops:
  7.2 219.2 %copy-start = (bf16[1,128,2048]{2,1,0:T(8,128)(2,1)S(1)}, bf16[1,128,2048]{2,1,0:T(8,128)(2,1)}, u32[]{:S(2)}) copy-start(bf16[1,128,2048]{2,1,0:T(8,128)(2,1)} %param.37) | copy-start | bytes 1572868
  7.2 94.0 %all-gather.3.cloned.1.call-start = ((), (), s32[]{:S(2)}) async-start(), calls=%async_computation.4 | async-start | bytes 3170304 | tf_op jit(solution)/shard_map/all_gather | solution.py:13
  8.6 172.0 %all-gather.5.cloned.1.call-start = ((), (), s32[]{:S(2)}) async-start(), calls=%async_computation.5 | async-start | bytes 1056768 | tf_op jit(solution)/shard_map/all_gather | solution.py:129
  17.0 3.1 %copy-start.7 = (s32[16,2]{0,1:T(2,128)S(1)}, s32[16,2]{0,1:T(2,128)}, u32[]{:S(2)}) copy-start(s32[16,2]{0,1:T(2,128)} %param.33) | copy-start | bytes 388
  17.0 3.4 %copy-start.8 = (f32[16,2]{0,1:T(2,128)S(1)}, f32[16,2]{0,1:T(2,128)}, u32[]{:S(2)}) copy-start(f32[16,2]{0,1:T(2,128)} %param.34) | copy-start | bytes 388
  17.0 84.2 %copy-start.2 = (bf16[16,2048]{1,0:T(8,128)(2,1)S(1)}, bf16[16,2048]{1,0:T(8,128)(2,1)}, u32[]{:S(2)}) copy-start(bf16[16,2048]{1,0:T(8,128)(2,1)} %param.19) | copy-start | bytes 196612
  17.0 84.2 %copy-start.5 = (f32[2048]{0:T(1024)S(1)}, f32[2048]{0:T(1024)}, u32[]{:S(2)}) copy-start(f32[2048]{0:T(1024)} %param.21) | copy-start | bytes 24580
  115.1 3.2 %copy-start.1 = (f32[16,4,64,64]{3,2,1,0:T(8,128)S(1)}, f32[16,4,64,64]{3,2,1,0:T(8,128)}, u32[]{:S(2)}) copy-start(f32[16,4,64,64]{3,2,1,0:T(8,128)} %get-tuple-element.10) | copy-start | bytes 3145732
  122.0 58.6 %copy-start.9 = (f32[256]{0:T(256)S(1)}, f32[256]{0:T(256)}, u32[]{:S(2)}) copy-start(f32[256]{0:T(256)} %param.30) | copy-start | bytes 3076
  126.1 66.8 %copy-start.6 = (f32[2048]{0:T(1024)S(1)}, f32[2048]{0:T(1024)}, u32[]{:S(2)}) copy-start(f32[2048]{0:T(1024)} %param.32) | copy-start | bytes 24580
  182.9 9.9 %all-to-all-start = ((bf16[4,16,2048]{2,1,0:T(8,128)(2,1)}), bf16[4,16,2048]{2,1,0:T(8,128)(2,1)S(1)}, u32[]{:S(2)}, u32[]{:S(2)}) async-start(bf16[4,16,2048]{2,1,0:T(8,128)(2,1)} %broadcast_in_dim.2), calls=%async_computation | async-start | bytes 524288 | tf_op jit(solution)/shard_map/all_to_all | solution.py:19
  194.8 31.1 %copy-start.3 = (bf16[1,2048,128]{2,1,0:T(8,128)(2,1)S(1)}, bf16[1,2048,128]{2,1,0:T(8,128)(2,1)}, u32[]{:S(2)}) copy-start(bf16[1,2048,128]{2,1,0:T(8,128)(2,1)} %param.35) | copy-start | bytes 1572868
  195.2 31.1 %copy-start.4 = (bf16[1,2048,128]{2,1,0:T(8,128)(2,1)S(1)}, bf16[1,2048,128]{2,1,0:T(8,128)(2,1)}, u32[]{:S(2)}) copy-start(bf16[1,2048,128]{2,1,0:T(8,128)(2,1)} %param.36) | copy-start | bytes 1572868
  241.2 18.6 %all-to-all-start.3 = ((bf16[128,2,256]{2,1,0:T(2,128)(2,1)}), bf16[128,2,256]{2,1,0:T(2,128)(2,1)S(1)}, u32[]{:S(2)}, u32[]{:S(2)}) async-start(bf16[128,2,256]{2,1,0:T(2,128)(2,1)} %reshape.134), calls=%async_computation.3 | async-start | bytes 262144 | tf_op jit(solution)/shard_map/all_to_all | solution.py:160
Sparse Core Ops, SparseCore 0:
  11.7 89.4 all-gather.2
  104.2 76.3 all-gather.4
where the time goes:
time: 268 us; the launch traced here: 267 us
  waiting for transfers between devices  154 us (57%)
  blocking collectives  42.4 us (16%)
  other arithmetic  18.1 us (7%)
  local copies, waits for them, and re-layouts  17.9 us (7%)
  between operations  14.3 us (5%)
  matrix products  11.1 us (4%)
  starting transfers between devices  9.82 us (4%)
    all_gather x1, waiting for transfers between devices, sent_together(): out = lax.all_gather(both, axis, axis=dim, tiled=True)  80.8 us
    all_gather x1, waiting for transfers between devices, body(): lax.all_gather(w_out, 'ep', axis=1, tiled=True)  54.1 us
    all_to_all x1, blocking collectives, body(): lax.all_to_all(outbound, 'ep', split_axis=0, concat_axis=0, tiled=True)  30.2 us
    all_to_all x1, waiting for transfers between devices, body(): lax.all_to_all(reduced.astype(jnp.bfloat16), 'ep', split_axis=0, concat_a...  12.8 us
    all_to_all x1, blocking collectives, sum_at_owner(): parts = lax.all_to_all(split_up(array, dim, peers), axis, 0, 0, tiled=True)  12.2 us
    mul x1, other arithmetic, recurrence(): removed[:, :, :, None] * (unit_keys * rate_heads)[:, :, None, :]  8.83 us
    all_to_all x1, starting transfers between devices, body(): lax.all_to_all(reduced.astype(jnp.bfloat16), 'ep', split_axis=0, concat_a...  5.77 us
    all_to_all x1, waiting for transfers between devices, from_everyone(): return lax.all_to_all(copies, axis, split_axis=0, concat_axis=0, tiled=True)  5.47 us
  transfers between devices with their start and end apart: 4, of which 4 were waited for; matrix products, arithmetic and copies ran while one was open for 14% of the time, Pallas kernels for 0%

commit v1 on v0

--- a/solution.py
+++ b/solution.py
@@ -126,7 +126,9 @@
     )
     partial_out = jnp.dot(
         head_out,
-        lax.all_gather(w_out, "ep", axis=1, tiled=True),
+        jnp.concatenate(
+            lax.all_to_all(jnp.stack([w_out] * lax.axis_size("ep")), "ep", 0, 0), axis=1
+        ),
         preferred_element_type=jnp.float32,
     )
     mixed_out = taken_together(partial_out.astype(jnp.bfloat16), "tp").astype(jnp.float32)

time: 268 us -> 226 us (0.84)
  waiting for transfers between devices: 154 us -> 91.1 us
  starting transfers between devices: 9.82 us -> 28.6 us
    all_gather x1 -> x0, waiting for transfers between devices: 54.1 us -> none  [body(): lax.all_gather(w_out, 'ep', axis=1, tiled=True)]
    all_to_all x0 -> x1, starting transfers between devices: none -> 18.9 us  [body(): lax.all_to_all(jnp.stack([w_out] * lax.axis_size('ep')), 'ep', 0, 0)]
    all_gather x1, waiting for transfers between devices: 80.8 us -> 72.8 us  [sent_together(): out = lax.all_gather(both, axis, axis=dim, tiled=True)]
  transfers between devices with their start and end apart: 4 -> 4, of which waited for: 4 -> 3; matrix products, arithmetic and copies ran while one was open for 14% -> 16% of each run, Pallas kernels for 0% -> 0%
where the time goes in v1:
time: 226 us; the launch traced here: 225 us
  waiting for transfers between devices  91.1 us (40%)
  blocking collectives  43.8 us (19%)
  starting transfers between devices  28.6 us (13%)
  local copies, waits for them, and re-layouts  19.7 us (9%)
  other arithmetic  17.3 us (8%)
  between operations  14.4 us (6%)
  matrix products  10.6 us (5%)
    all_gather x1, waiting for transfers between devices, sent_together(): out = lax.all_gather(both, axis, axis=dim, tiled=True)  72.8 us
    all_to_all x1, blocking collectives, body(): lax.all_to_all(outbound, 'ep', split_axis=0, concat_axis=0, tiled=True)  31.6 us
    all_to_all x1, starting transfers between devices, body(): lax.all_to_all(jnp.stack([w_out] * lax.axis_size('ep')), 'ep', 0, 0)  18.9 us
    all_to_all x1, waiting for transfers between devices, body(): lax.all_to_all(reduced.astype(jnp.bfloat16), 'ep', split_axis=0, concat_a...  12.8 us
    all_to_all x1, blocking collectives, sum_at_owner(): parts = lax.all_to_all(split_up(array, dim, peers), axis, 0, 0, tiled=True)  12.2 us
    mul x1, other arithmetic, recurrence(): removed[:, :, :, None] * (unit_keys * rate_heads)[:, :, None, :]  8.83 us
    all_to_all x1, starting transfers between devices, body(): lax.all_to_all(reduced.astype(jnp.bfloat16), 'ep', split_axis=0, concat_a...  5.77 us
    all_to_all x1, waiting for transfers between devices, from_everyone(): return lax.all_to_all(copies, axis, split_axis=0, concat_axis=0, tiled=True)  5.47 us
  transfers between devices with their start and end apart: 4, of which 3 were waited for; matrix products, arithmetic and copies ran while one was open for 16% of the time, Pallas kernels for 0%

profile of v1, /device:TPU:1, one launch (start us, length us, event | category | flops | bytes accessed | tf_op | source)
XLA Modules:
  0.0 225.5 jit_solution(3566104951445410757)
XLA Ops:
  7.3 1.4 pad_maximum_fusion
  8.7 1.8 stack.2
  10.5 18.9 %all-to-all-start = ((bf16[128,256,16]{1,2,0:T(8,128)(2,1)}), bf16[128,256,16]{1,2,0:T(8,128)(2,1)}, u32[]{:S(2)}, u32[]{:S(2)}) async-start(bf16[128,256,16]{1,2,0:T(8,128)(2,1)} %stack.2), calls=%async_computation | async-start | bytes 2097152 | tf_op jit(solution)/shard_map/all_to_all | solution.py:130
  29.5 1.1 fusion.10
  30.8 1.2 fusion.55
  32.0 2.1 reshape.164
  34.2 1.5 mul.214
  35.7 3.0 %mul.234 = f32[16,4,4096]{2,1,0:T(4,128)} reshape(f32[16,4,64,64]{3,2,1,0:T(8,128)} %mul.214) | data formatting | bytes 2097152 | tf_op jit(solution)/shard_map/mul | solution.py:68
  39.2 72.8 %all-gather.2.cloned.1.call-done = bf16[2048,768]{1,0:T(8,128)(2,1)} async-done(((bf16[16,768]{1,0:T(8,128)(2,1)}), bf16[2048,768]{1,0:T(8,128)(2,1)}) %all-gather.2.cloned.1.call-update) | async-done | bytes 3145744 | tf_op jit(solution)/shard_map/all_gather | solution.py:13
  111.9 1.5 fusion.14
  113.5 1.5 fusion.12
  115.1 1.5 fusion.13
  116.9 8.8 %broadcast_multiply_fusion = (f32[16,4,64,64]{3,2,1,0:T(8,128)}, f32[16,4,64]{2,1,0:T(4,128)S(1)}, f32[16,4,64,64]{3,2,1,0:T(8,128)}) fusion(f32[16,4,64]{2,1,0:T(4,128)S(1)} %reshape.175, f32[16,4,64]{2,1,0:T(4,128)S(1)} %reshape.176, f32[16,4,64]{2,1,0:T(4,128)S(1)} %reshape.177, f32[16,4,64,64]{3,2,1,0:T(8,128)S(1)} %reshape.164, ...), kind=kOutput, calls=%fused_computation.33 | output fusion | flops 2097215 | bytes 3260416 | tf_op jit(solution)/shard_map/mul | solution.py:69
  125.8 3.2 %mul.236 = f32[16,4,4096]{2,1,0:T(4,128)} reshape(f32[16,4,64,64]{3,2,1,0:T(8,128)} %get-tuple-element.12) | data formatting | bytes 2097152 | tf_op jit(solution)/shard_map/mul | solution.py:69
  128.9 1.8 mul.237
  130.9 1.8 mul.238
  132.7 4.1 %multiply_reduce_fusion.2 = (f32[16,4]{1,0:T(8,128)S(1)}, f32[16,4,4096]{2,1,0:T(4,128)}) fusion(f32[16,4,4096]{2,1,0:T(4,128)} %mul.238, f32[16,4,4096]{2,1,0:T(4,128)} %mul.237, f32[16,4,4096]{2,1,0:T(4,128)} %mul.236, f32[16,4,4096]{2,1,0:T(4,128)} %param.20, f32[16,4,4096]{2,1,0:T(4,128)} %mul.234), kind=kLoop, calls=%fused_computation.31 | loop fusion | flops 1310656 | bytes 6291712 | tf_op jit(solution)/shard_map/reduce_sum | solution.py:73
  137.2 1.6 convolution_convert_fusion.2
  138.8 0.7 broadcast_in_dim.2
  139.5 4.0 %all-to-all-start.1 = ((bf16[4,16,2048]{2,1,0:T(8,128)(2,1)}), bf16[4,16,2048]{2,1,0:T(8,128)(2,1)S(1)}, u32[]{:S(2)}, u32[]{:S(2)}) async-start(bf16[4,16,2048]{2,1,0:T(8,128)(2,1)} %broadcast_in_dim.2), calls=%async_computation.1 | async-start | bytes 524288 | tf_op jit(solution)/shard_map/all_to_all | solution.py:19
  143.9 5.5 %all-to-all-done.1 = bf16[4,16,2048]{2,1,0:T(8,128)(2,1)S(1)} async-done(((bf16[4,16,2048]{2,1,0:T(8,128)(2,1)}), bf16[4,16,2048]{2,1,0:T(8,128)(2,1)S(1)}, u32[]{:S(2)}, u32[]{:S(2)}) %all-to-all-start.1) | async-done | bytes 262176 | tf_op jit(solution)/shard_map/all_to_all | solution.py:19
  149.9 0.5 broadcast.136
  150.5 1.0 reduce.4
  151.9 31.6 %all_to_all.25 = bf16[128,2,1024]{2,1,0:T(2,128)(2,1)S(1)} all-to-all(bf16[128,2,1024]{2,1,0:T(2,128)(2,1)S(1)} %reshape.179), channel_id=1, replica_groups=mesh['ep'=128,'tp'=4] {'ep'}, dimensions={0} | all-to-all | bytes 1048576 | tf_op jit(solution)/shard_map/all_to_all | solution.py:152
  183.4 0.4 reshape.180
  184.3 0.7 convolution_convert_fusion
  185.5 12.2 %all_to_all.26 = bf16[4,128,1,512]{3,1,2,0:T(8,128)(2,1)S(1)} all-to-all(bf16[4,128,1,512]{3,1,2,0:T(8,128)(2,1)S(1)} %bitcast.42), channel_id=1, replica_groups=mesh['ep'=128,'tp'=4] {'tp'}, dimensions={0} | all-to-all | bytes 1048576 | tf_op jit(solution)/shard_map/all_to_all | solution.py:34
  197.8 0.7 reduce.5
  198.5 0.7 reshape.181
  199.2 5.8 %all-to-all-start.4 = ((bf16[128,2,256]{2,1,0:T(2,128)(2,1)}), bf16[128,2,256]{2,1,0:T(2,128)(2,1)S(1)}, u32[]{:S(2)}, u32[]{:S(2)}) async-start(bf16[128,2,256]{2,1,0:T(2,128)(2,1)} %reshape.181), calls=%async_computation.4 | async-start | bytes 262144 | tf_op jit(solution)/shard_map/all_to_all | solution.py:162
  205.0 12.8 %all-to-all-done.4 = bf16[128,2,256]{2,1,0:T(2,128)(2,1)S(1)} async-done(((bf16[128,2,256]{2,1,0:T(2,128)(2,1)}), bf16[128,2,256]{2,1,0:T(2,128)(2,1)S(1)}, u32[]{:S(2)}, u32[]{:S(2)}) %all-to-all-start.4) | async-done | bytes 131104 | tf_op jit(solution)/shard_map/all_to_all | solution.py:162
  217.9 0.8 fusion.7
  (67 shorter events, 4.1 us)
Async XLA Ops:
  7.2 177.2 %copy-start = (bf16[1,128,2048]{2,1,0:T(8,128)(2,1)S(1)}, bf16[1,128,2048]{2,1,0:T(8,128)(2,1)}, u32[]{:S(2)}) copy-start(bf16[1,128,2048]{2,1,0:T(8,128)(2,1)} %param.37) | copy-start | bytes 1572868
  7.2 22.2 %copy-start.2 = (bf16[16,2048]{1,0:T(8,128)(2,1)S(1)}, bf16[16,2048]{1,0:T(8,128)(2,1)}, u32[]{:S(2)}) copy-start(bf16[16,2048]{1,0:T(8,128)(2,1)} %param.19) | copy-start | bytes 196612
  7.2 22.3 %copy-start.7 = (f32[2048]{0:T(1024)S(1)}, f32[2048]{0:T(1024)}, u32[]{:S(2)}) copy-start(f32[2048]{0:T(1024)} %param.21) | copy-start | bytes 24580
  7.2 22.3 %copy-start.5 = (bf16[2048,64]{0,1:T(8,128)(2,1)S(1)}, bf16[2048,64]{0,1:T(8,128)(2,1)}, u32[]{:S(2)}) copy-start(bf16[2048,64]{0,1:T(8,128)(2,1)} %param.28) | copy-start | bytes 786436
  7.2 23.6 %copy-start.6 = (bf16[2048,64]{0,1:T(8,128)(2,1)S(1)}, bf16[2048,64]{0,1:T(8,128)(2,1)}, u32[]{:S(2)}) copy-start(bf16[2048,64]{0,1:T(8,128)(2,1)} %param.25) | copy-start | bytes 786436
  7.2 23.6 %copy-start.11 = (f32[256]{0:T(256)S(1)}, f32[256]{0:T(256)}, u32[]{:S(2)}) copy-start(f32[256]{0:T(256)} %param.27) | copy-start | bytes 3076
  7.2 104.7 %all-gather.2.cloned.1.call-start = ((), (), s32[]{:S(2)}) async-start(), calls=%async_computation.5 | async-start | bytes 3170304 | tf_op jit(solution)/shard_map/all_gather | solution.py:13
  10.5 126.7 %all-to-all-start = ((bf16[128,256,16]{1,2,0:T(8,128)(2,1)}), bf16[128,256,16]{1,2,0:T(8,128)(2,1)}, u32[]{:S(2)}, u32[]{:S(2)}) async-start(bf16[128,256,16]{1,2,0:T(8,128)(2,1)} %stack.2), calls=%async_computation | async-start | bytes 2097152 | tf_op jit(solution)/shard_map/all_to_all | solution.py:130
  35.7 3.1 %copy-start.12 = (f32[256]{0:T(256)S(1)}, f32[256]{0:T(256)}, u32[]{:S(2)}) copy-start(f32[256]{0:T(256)} %param.30) | copy-start | bytes 3076
  35.7 3.1 %copy-start.9 = (s32[16,2]{0,1:T(2,128)S(1)}, s32[16,2]{0,1:T(2,128)}, u32[]{:S(2)}) copy-start(s32[16,2]{0,1:T(2,128)} %param.33) | copy-start | bytes 388
  35.7 3.4 %copy-start.10 = (f32[16,2]{0,1:T(2,128)S(1)}, f32[16,2]{0,1:T(2,128)}, u32[]{:S(2)}) copy-start(f32[16,2]{0,1:T(2,128)} %param.34) | copy-start | bytes 388
  125.8 3.2 %copy-start.1 = (f32[16,4,64,64]{3,2,1,0:T(8,128)S(1)}, f32[16,4,64,64]{3,2,1,0:T(8,128)}, u32[]{:S(2)}) copy-start(f32[16,4,64,64]{3,2,1,0:T(8,128)} %get-tuple-element.10) | copy-start | bytes 3145732
  136.8 12.8 %copy-start.8 = (f32[2048]{0:T(1024)S(1)}, f32[2048]{0:T(1024)}, u32[]{:S(2)}) copy-start(f32[2048]{0:T(1024)} %param.32) | copy-start | bytes 24580
  139.5 9.9 %all-to-all-start.1 = ((bf16[4,16,2048]{2,1,0:T(8,128)(2,1)}), bf16[4,16,2048]{2,1,0:T(8,128)(2,1)S(1)}, u32[]{:S(2)}, u32[]{:S(2)}) async-start(bf16[4,16,2048]{2,1,0:T(8,128)(2,1)} %broadcast_in_dim.2), calls=%async_computation.1 | async-start | bytes 524288 | tf_op jit(solution)/shard_map/all_to_all | solution.py:19
  151.5 32.4 %copy-start.3 = (bf16[1,2048,128]{2,1,0:T(8,128)(2,1)S(1)}, bf16[1,2048,128]{2,1,0:T(8,128)(2,1)}, u32[]{:S(2)}) copy-start(bf16[1,2048,128]{2,1,0:T(8,128)(2,1)} %param.35) | copy-start | bytes 1572868
  151.8 32.5 %copy-start.4 = (bf16[1,2048,128]{2,1,0:T(8,128)(2,1)S(1)}, bf16[1,2048,128]{2,1,0:T(8,128)(2,1)}, u32[]{:S(2)}) copy-start(bf16[1,2048,128]{2,1,0:T(8,128)(2,1)} %param.36) | copy-start | bytes 1572868
  199.2 18.6 %all-to-all-start.4 = ((bf16[128,2,256]{2,1,0:T(2,128)(2,1)}), bf16[128,2,256]{2,1,0:T(2,128)(2,1)S(1)}, u32[]{:S(2)}, u32[]{:S(2)}) async-start(bf16[128,2,256]{2,1,0:T(2,128)(2,1)} %reshape.181), calls=%async_computation.4 | async-start | bytes 262144 | tf_op jit(solution)/shard_map/all_to_all | solution.py:162
Sparse Core Ops, SparseCore 0:
  11.7 100.1 all-gather.1
